TPU v7x, 32 devices: a whole 2x2x4 slice. The times are simulated.
32 devices in a mesh: rep: 2 (over x), fs: 8 (over z, y), tp: 2 (over core).
Axes of the slice: x: 2, y: 2, z: 4, core: 2. Of those that a mesh axis runs over, the one named last changes fastest.
Arguments:
- tokens: bfloat16 [4096, 2048], P(('rep', 'fs')), may hold values from -6 to 6
- mid_tokens: bfloat16 [4096, 2048], P(('rep', 'fs')), may hold values from -6 to 6
- out_grad: bfloat16 [4096, 2048], P(('rep', 'fs')), may hold values from -6 to 6
- gate_first: bfloat16 [2048, 3072], P('fs', 'tp'), may hold values from -0.125 to 0.125
- up_first: bfloat16 [2048, 3072], P('fs', 'tp'), may hold values from -0.125 to 0.125
- down_first: bfloat16 [3072, 2048], P('tp', 'fs'), may hold values from -0.109375 to 0.109375
- gate_second: bfloat16 [2048, 3072], P('fs', 'tp'), may hold values from -0.125 to 0.125
- up_second: bfloat16 [2048, 3072], P('fs', 'tp'), may hold values from -0.125 to 0.125
- down_second: bfloat16 [3072, 2048], P('tp', 'fs'), may hold values from -0.109375 to 0.109375
Outputs:
- input_grad: bfloat16 [4096, 2048], P(('rep', 'fs'))
- down_grad: float32 [3072, 2048], P('tp', 'fs')
- row_norms: float32 [3072], P('tp')
All inputs are finite; a program needn't handle non-finite values.
Results may differ from a plain program's by a relative error of at most 0.025.
Values may be sent and summed in bfloat16 or wider, within the bound.
A program may use at most 128 MiB of HBM per device.

v0:
```python
import jax
import jax.numpy as jnp
from jax import lax
from jax.sharding import PartitionSpec as P

eps = 1e-06


def gathered(gate_w, up_w, down_w):
    half = gate_w.shape[1] // lax.axis_size("rep")
    start = lax.axis_index("rep") * half
    own = jnp.concatenate(
        [
            lax.dynamic_slice_in_dim(gate_w, start, half, 1),
            lax.dynamic_slice_in_dim(up_w, start, half, 1),
            lax.dynamic_slice_in_dim(down_w, start, half, 0).T,
        ],
        axis=1,
    )
    return lax.all_gather(own, "fs", axis=0, tiled=True)


def half_back(field, fields, carried, carrieds, weights):
    half = weights.shape[1] // 3
    wide = fields.astype(jnp.float32)
    normed_b = (wide * lax.rsqrt(jnp.mean(wide * wide, axis=1, keepdims=True) + eps)).astype(
        jnp.bfloat16
    )
    gates, uppers, downs = (weights[:, i * half : (i + 1) * half] for i in range(3))
    gate = jnp.dot(normed_b, gates, preferred_element_type=jnp.float32)
    upper = jnp.dot(normed_b, uppers, preferred_element_type=jnp.float32)
    back = 0.5 * jnp.dot(carrieds, downs, preferred_element_type=jnp.float32)
    logistic = jax.nn.sigmoid(gate)
    activated = gate * logistic
    hidden = (activated * upper).astype(jnp.bfloat16)
    d_gate = (back * upper * logistic * (1.0 + gate * (1.0 - logistic))).astype(jnp.bfloat16)
    d_up = (back * activated).astype(jnp.bfloat16)
    dims = (((1,), (1,)), ((), ()))
    partial_sum = lax.dot_general(d_gate, gates, dims, preferred_element_type=jnp.float32)
    partial_sum = partial_sum + lax.dot_general(
        d_up, uppers, dims, preferred_element_type=jnp.float32
    )
    partial_sum = partial_sum.astype(jnp.bfloat16)
    n = field.shape[0]
    reps = lax.axis_size("rep")
    me = lax.axis_index("rep")
    total = lax.dynamic_slice_in_dim(partial_sum, me * n, n, 0).astype(jnp.float32)
    for k in range(1, reps):
        other = lax.rem(me + k, reps)
        sent = lax.dynamic_slice_in_dim(partial_sum, other * n, n, 0)
        got = lax.ppermute(sent, "rep", [(i, (i + k) % reps) for i in range(reps)])
        total = total + got.astype(jnp.float32)
    d_normed = lax.psum(total.astype(jnp.bfloat16), "tp").astype(jnp.float32)
    own = field.astype(jnp.float32)
    scale = lax.rsqrt(jnp.mean(own * own, axis=1, keepdims=True) + eps)
    normed = own * scale
    d_field = carried.astype(jnp.float32) + scale * (
        d_normed - normed * jnp.mean(d_normed * normed, axis=1, keepdims=True)
    )
    return (d_field.astype(jnp.bfloat16), hidden)


def over_rep(x):
    return lax.all_gather(x, "rep", axis=0, tiled=True)


def on_device(
    tokens,
    mid_tokens,
    out_grad,
    gate_first,
    up_first,
    down_first,
    gate_second,
    up_second,
    down_second,
):
    second = gathered(gate_second, up_second, down_second)
    first = gathered(gate_first, up_first, down_first)
    mid_grad, _ = half_back(mid_tokens, over_rep(mid_tokens), out_grad, over_rep(out_grad), second)
    mid_grads = over_rep(mid_grad)
    d_input, hidden = half_back(tokens, over_rep(tokens), mid_grad, mid_grads, first)
    partial = lax.dot_general(
        mid_grads, hidden, (((0,), (0,)), ((), ())), preferred_element_type=jnp.float32
    )
    shard = lax.psum_scatter(
        (0.5 * partial).astype(jnp.bfloat16), "fs", scatter_dimension=0, tiled=True
    )
    grad = lax.all_gather(shard, "rep", axis=1, tiled=True).astype(jnp.float32)
    norms = lax.psum(jnp.sum(grad * grad, axis=0), "fs")
    return (d_input, grad.T, norms)


def solution(mesh):
    placed = (
        P(("rep", "fs"), None),
        P(("rep", "fs"), None),
        P(("rep", "fs"), None),
        P("fs", "tp"),
        P("fs", "tp"),
        P("tp", "fs"),
        P("fs", "tp"),
        P("fs", "tp"),
        P("tp", "fs"),
    )
    return jax.shard_map(
        on_device,
        mesh=mesh,
        in_specs=placed,
        out_specs=(P(("rep", "fs"), None), P("tp", "fs"), P("tp")),
        check_vma=False,
    )
```

profile of v0, /device:TPU:0, one launch (start us, length us, event | category | flops | bytes accessed | tf_op | source)
XLA Modules:
  0.0 675.1 jit_solution(365070415602245520)
XLA Ops:
  11.5 33.9 %all-gather.11.cloned.1.call-done = bf16[512,2048]{1,0:T(8,128)(2,1)} async-done(((bf16[256,2048]{1,0:T(8,128)(2,1)}), bf16[512,2048]{1,0:T(8,128)(2,1)}) %all-gather.11.cloned.1.call-update) | async-done | bytes 2097168 | tf_op jit(solution)/shard_map/all_gather | solution.py:64
  47.6 138.2 %all-gather.7.cloned.1.call-done = bf16[2048,2304]{0,1:T(8,128)(2,1)} async-done(((bf16[256,2304]{0,1:T(8,128)(2,1)}), bf16[2048,2304]{0,1:T(8,128)(2,1)}) %all-gather.7.cloned.1.call-update) | async-done | bytes 9437200 | tf_op jit(solution)/shard_map/all_gather | solution.py:20
  185.8 4.9 fusion.17
  190.7 27.9 %all-gather.9.cloned.1.call-done = bf16[512,2048]{1,0:T(8,128)(2,1)} async-done(((bf16[256,2048]{1,0:T(8,128)(2,1)}), bf16[512,2048]{1,0:T(8,128)(2,1)}) %all-gather.9.cloned.1.call-update) | async-done | bytes 2097168 | tf_op jit(solution)/shard_map/all_gather | solution.py:64
  218.6 5.5 fusion.42
  224.1 9.8 %fusion.15 = f32[512,2048]{1,0:T(8,128)} fusion(bf16[2048,2304]{0,1:T(8,128)(2,1)} %all-gather.7.cloned.1.call-done, f32[768,512]{1,0:T(8,128)} %fusion.42, f32[512,768]{0,1:T(8,128)} %fusion.17, bf16[512,2048]{1,0:T(8,128)(2,1)S(1)} %copy-done.8, f32[512]{0:T(512)S(1)} %add_rsqrt_fusion.1), kind=kOutput, calls=%fused_computation.22 | convolution fusion | flops 3228303360 | bytes 15730688 | tf_op jit(solution)/shard_map/dot_general | solution.py:39
  233.9 6.0 add_convert_fusion.1
  241.3 24.7 %collective-permute-done = bf16[256,2048]{1,0:T(8,128)(2,1)} collective-permute-done((bf16[256,2048]{1,0:T(8,128)(2,1)}, bf16[256,2048]{1,0:T(8,128)(2,1)}, u32[]{:S(2)}, u32[]{:S(2)}) %collective-permute-start) | collective-permute-done | bytes 1048608 | tf_op jit(solution)/shard_map/ppermute | solution.py:51
  266.0 2.6 add_convert_fusion.3
  272.7 15.5 %all-reduce.3.cloned.1.call-done = bf16[256,2048]{1,0:T(8,128)(2,1)} async-done(((bf16[256,2048]{1,0:T(8,128)(2,1)}), bf16[256,2048]{1,0:T(8,128)(2,1)}) %all-reduce.3.cloned.1.call-update) | async-done | bytes 1048592 | tf_op jit(solution)/shard_map/psum | solution.py:53
  291.9 32.0 %all-gather.17.cloned.1.call-done = bf16[512,2048]{1,0:T(8,128)(2,1)} async-done(((bf16[256,2048]{1,0:T(8,128)(2,1)}), bf16[512,2048]{1,0:T(8,128)(2,1)}) %all-gather.17.cloned.1.call-update) | async-done | bytes 2097168 | tf_op jit(solution)/shard_map/all_gather | solution.py:64
  326.1 138.0 %all-gather.15.cloned.1.call-done = bf16[2048,2304]{0,1:T(8,128)(2,1)} async-done(((bf16[256,2304]{0,1:T(8,128)(2,1)}), bf16[2048,2304]{0,1:T(8,128)(2,1)}) %all-gather.15.cloned.1.call-update) | async-done | bytes 9437200 | tf_op jit(solution)/shard_map/all_gather | solution.py:20
  464.1 4.9 fusion.10
  469.0 5.2 fusion.13
  474.3 23.3 %all-gather.13.cloned.1.call-done = bf16[512,2048]{1,0:T(8,128)(2,1)} async-done(((bf16[256,2048]{1,0:T(8,128)(2,1)}), bf16[512,2048]{1,0:T(8,128)(2,1)}) %all-gather.13.cloned.1.call-update) | async-done | bytes 2097168 | tf_op jit(solution)/shard_map/all_gather | solution.py:64
  497.5 4.5 fusion.45
  502.0 4.1 fusion.8
  506.2 4.0 add_convert_fusion
  510.7 24.4 %collective-permute-done.1 = bf16[256,2048]{1,0:T(8,128)(2,1)S(1)} collective-permute-done((bf16[256,2048]{1,0:T(8,128)(2,1)S(1)}, bf16[256,2048]{1,0:T(8,128)(2,1)S(1)}, u32[]{:S(2)}, u32[]{:S(2)}) %collective-permute-start.1) | collective-permute-done | bytes 1048608 | tf_op jit(solution)/shard_map/ppermute | solution.py:51
  536.7 5.5 multiply_convert_fusion
  543.8 12.2 %all-reduce.5.cloned.1.call-done = bf16[256,2048]{1,0:T(8,128)(2,1)} async-done(((bf16[256,2048]{1,0:T(8,128)(2,1)}), bf16[256,2048]{1,0:T(8,128)(2,1)}) %all-reduce.5.cloned.1.call-update) | async-done | bytes 1048592 | tf_op jit(solution)/shard_map/psum | solution.py:53
  559.5 75.6 %reduce-scatter.2.cloned.1.call-done = bf16[256,768]{1,0:T(8,128)(2,1)} async-done(((bf16[2048,768]{1,0:T(8,128)(2,1)}), bf16[256,768]{1,0:T(8,128)(2,1)}) %reduce-scatter.2.cloned.1.call-update) | async-done | bytes 393232 | tf_op jit(solution)/shard_map/reduce_scatter | solution.py:86
  635.1 11.0 %all_gather.27 = bf16[256,1536]{1,0:T(8,128)(2,1)S(1)} all-gather(bf16[256,768]{1,0:T(8,128)(2,1)} %reduce-scatter.2.cloned.1.call-done), channel_id=1, replica_groups=mesh['rep'=2,'fs'=8,'tp'=2] {'rep'}, dimensions={1}, use_global_device_ids=true | all-gather | bytes 1179648 | tf_op jit(solution)/shard_map/all_gather | solution.py:89
  648.1 20.5 %psum.23 = f32[1536]{0:T(1024)} all-reduce(f32[1536]{0:T(1024)S(1)} %fusion.34), channel_id=1, replica_groups=mesh['rep'=2,'fs'=8,'tp'=2] {'fs'}, use_global_device_ids=true, to_apply=%region_10.0 | all-reduce | flops 1536 | bytes 12288 | tf_op jit(solution)/shard_map/psum | solution.py:90
  (78 shorter events, 26.9 us)
Async XLA Ops:
  7.2 2.3 copy-start
  7.2 38.2 %all-gather.11.cloned.1.call-start = ((), (), s32[]{:S(2)}) async-start(), calls=%async_computation.3 | async-start | bytes 3145728 | tf_op jit(solution)/shard_map/all_gather | solution.py:64
  7.9 177.9 %all-gather.7.cloned.1.call-start = ((), (), s32[]{:S(2)}) async-start(), calls=%async_computation.1 | async-start | bytes 10616832 | tf_op jit(solution)/shard_map/all_gather | solution.py:20
  10.7 208.0 %all-gather.9.cloned.1.call-start = ((), (), s32[]{:S(2)}) async-start(), calls=%async_computation.2 | async-start | bytes 3145728 | tf_op jit(solution)/shard_map/all_gather | solution.py:64
  11.4 276.8 %all-reduce.3.cloned.1.call-start = ((), (), s32[]{:S(2)}) async-start(), calls=%async_computation.4 | async-start | bytes 2097152 | tf_op jit(solution)/shard_map/psum | solution.py:53
  45.4 140.4 %copy-start.8 = (bf16[512,2048]{1,0:T(8,128)(2,1)S(1)}, bf16[512,2048]{1,0:T(8,128)(2,1)}, u32[]{:S(2)}) copy-start(bf16[512,2048]{1,0:T(8,128)(2,1)} %all-gather.11.cloned.1.call-done) | copy-start | bytes 6291460
  240.9 25.1 %collective-permute-start = (bf16[256,2048]{1,0:T(8,128)(2,1)}, bf16[256,2048]{1,0:T(8,128)(2,1)}, u32[]{:S(2)}, u32[]{:S(2)}) collective-permute-start(bf16[256,2048]{1,0:T(8,128)(2,1)} %constant_dynamic-slice_fusion.3), channel_id=1, source_target_pairs={{0,16},{16,0},{1,17},{17,1},{2,18},{18,2},{3,19},{19,3},{4,20},{20... | collective-permute-start | bytes 3145736 | tf_op jit(solution)/shard_map/ppermute | solution.py:51
  268.6 2.2 copy-start.10
  268.6 55.3 %all-gather.17.cloned.1.call-start = ((), (), s32[]{:S(2)}) async-start(), calls=%async_computation.7 | async-start | bytes 3145728 | tf_op jit(solution)/shard_map/all_gather | solution.py:64
  269.2 194.9 %all-gather.15.cloned.1.call-start = ((), (), s32[]{:S(2)}) async-start(), calls=%async_computation.6 | async-start | bytes 10616832 | tf_op jit(solution)/shard_map/all_gather | solution.py:20
  270.8 1.7 copy-start.2
  271.9 18.1 %copy-start.7 = (bf16[256,2048]{1,0:T(8,128)(2,1)S(1)}, bf16[256,2048]{1,0:T(8,128)(2,1)}, u32[]{:S(2)}) copy-start(bf16[256,2048]{1,0:T(8,128)(2,1)} %param.11) | copy-start | bytes 3145732
  271.9 225.6 %all-gather.13.cloned.1.call-start = ((), (), s32[]{:S(2)}) async-start(), calls=%async_computation.5 | async-start | bytes 3145728 | tf_op jit(solution)/shard_map/all_gather | solution.py:64
  288.2 1.8 copy-start.5
  291.6 264.4 %all-reduce.5.cloned.1.call-start = ((), (), s32[]{:S(2)}) async-start(), calls=%async_computation.8 | async-start | bytes 2097152 | tf_op jit(solution)/shard_map/psum | solution.py:53
  323.9 140.2 %copy-start.9 = (bf16[512,2048]{1,0:T(8,128)(2,1)S(1)}, bf16[512,2048]{1,0:T(8,128)(2,1)}, u32[]{:S(2)}) copy-start(bf16[512,2048]{1,0:T(8,128)(2,1)} %all-gather.17.cloned.1.call-done) | copy-start | bytes 6291460
  474.3 27.7 %copy-start.12 = (f32[512,768]{0,1:T(8,128)S(1)}, f32[512,768]{0,1:T(8,128)}, u32[]{:S(2)}) copy-start(f32[512,768]{0,1:T(8,128)} %fusion.10) | copy-start | bytes 4718596
  497.5 4.5 copy-start.13
  510.2 26.5 %copy-start.11 = (bf16[512,2048]{1,0:T(8,128)(2,1)S(1)}, bf16[512,2048]{1,0:T(8,128)(2,1)}, u32[]{:S(2)}) copy-start(bf16[512,2048]{1,0:T(8,128)(2,1)} %all-gather.13.cloned.1.call-done) | copy-start | bytes 6291460
  510.2 24.8 %collective-permute-start.1 = (bf16[256,2048]{1,0:T(8,128)(2,1)S(1)}, bf16[256,2048]{1,0:T(8,128)(2,1)S(1)}, u32[]{:S(2)}, u32[]{:S(2)}) collective-permute-start(bf16[256,2048]{1,0:T(8,128)(2,1)S(1)} %constant_dynamic-slice_fusion), channel_id=1, source_target_pairs={{0,16},{16,0},{1,17},{17,1},{2,18},{18,2},{3,19},{19,3},{4,20},{20... | collective-permute-start | bytes 3145736 | tf_op jit(solution)/shard_map/ppermute | solution.py:51
  536.5 98.7 %reduce-scatter.2.cloned.1.call-start = ((), (), s32[]{:S(2)}) async-start(), calls=%async_computation.9 | async-start | bytes 3538944 | tf_op jit(solution)/shard_map/reduce_scatter | solution.py:86
  543.5 14.4 %copy-start.4 = (bf16[256,2048]{1,0:T(8,128)(2,1)S(1)}, bf16[256,2048]{1,0:T(8,128)(2,1)}, u32[]{:S(2)}) copy-start(bf16[256,2048]{1,0:T(8,128)(2,1)} %fusion.28) | copy-start | bytes 3145732
  556.0 1.8 copy-start.6
  646.1 22.4 %copy-start.1 = (bf16[1536,256]{1,0:T(8,128)(2,1)S(1)}, bf16[1536,256]{1,0:T(8,128)(2,1)}, u32[]{:S(2)}) copy-start(bf16[1536,256]{1,0:T(8,128)(2,1)} %param.17) | copy-start | bytes 2359300
  (1 other events, 1.3 us)
Sparse Core Ops, SparseCore 0:
  9.5 35.8 all-gather.10
  48.0 137.7 all-gather.6
  187.3 31.2 all-gather.8
  268.7 19.4 all-reduce.2
  289.5 34.2 all-gather.16
  326.3 137.7 all-gather.14
  466.2 31.2 all-gather.12
  536.6 19.4 all-reduce.4
  559.6 75.4 reduce-scatter.1
where the time goes:
time: 676 us; the launch traced here: 675 us
  waiting for transfers between devices  548 us (81%)
  matrix products  54.4 us (8%)
  blocking collectives  31.5 us (5%)
  other arithmetic  18.4 us (3%)
  between operations  14.1 us (2%)
  local copies, waits for them, and re-layouts  7.56 us (1%)
    all_gather x2, waiting for transfers between devices, gathered(): return lax.all_gather(own, 'fs', axis=0, tiled=True)  276 us
    all_gather x4, waiting for transfers between devices, over_rep(): return lax.all_gather(x, 'rep', axis=0, tiled=True)  117 us
    reduce_scatter x1, waiting for transfers between devices, on_device(): lax.psum_scatter((0.5 * partial).astype(jnp.bfloat16), 'fs', scatter_dime...  75.6 us
    ppermute x2, waiting for transfers between devices, half_back(): got = lax.ppermute(sent, 'rep', [(i, (i + k) % reps) for i in range(reps)])  49.1 us
    psum x2, waiting for transfers between devices, half_back(): d_normed = lax.psum(total.astype(jnp.bfloat16), 'tp').astype(jnp.float32)  27.7 us
    psum x1, blocking collectives, on_device(): norms = lax.psum(jnp.sum(grad * grad, axis=0), 'fs')  20.5 us
    dot_general x2, matrix products, half_back(): lax.dot_general(d_gate, gates, dims, preferred_element_type=jnp.float32)  13.9 us
  transfers between devices with their start and end apart: 11, of which 11 were waited for; matrix products, arithmetic and copies ran while one was open for 6% of the time, Pallas kernels for 0%

commit v1 on v0

--- a/solution.py
+++ b/solution.py
@@ -4,6 +4,13 @@
 from jax.sharding import PartitionSpec as P
 
 eps = 1e-06
+
+
+def exchange_gather(array, mesh_axis, d):
+    devices = lax.axis_size(mesh_axis)
+    shards = jnp.stack([array for _ in range(devices)])
+    shards = lax.all_to_all(shards, mesh_axis, split_axis=0, concat_axis=0)
+    return jnp.concatenate(shards, axis=d)
 
 
 def gathered(gate_w, up_w, down_w):
@@ -61,7 +68,7 @@
 
 
 def over_rep(x):
-    return lax.all_gather(x, "rep", axis=0, tiled=True)
+    return exchange_gather(x, "rep", 0)
 
 
 def on_device(

time: 676 us -> 554 us (0.82)
  waiting for transfers between devices: 548 us -> 396 us
  starting transfers between devices: 1.53 us -> 21.3 us
  other arithmetic: 18.4 us -> 25.2 us
    all_gather x4 -> x0, waiting for transfers between devices: 117 us -> none  [over_rep(): return lax.all_gather(x, 'rep', axis=0, tiled=True)]
    all_gather x2, waiting for transfers between devices: 276 us -> 218 us  [gathered(): return lax.all_gather(own, 'fs', axis=0, tiled=True)]
    all_to_all x0 -> x4, waiting for transfers between devices: none -> 45.8 us  [exchange_gather(): shards = lax.all_to_all(shards, mesh_axis, split_axis=0, concat_axis=0)]
    all_to_all x0 -> x4, starting transfers between devices: none -> 17.8 us  [exchange_gather(): shards = lax.all_to_all(shards, mesh_axis, split_axis=0, concat_axis=0)]
    psum x2, waiting for transfers between devices: 27.7 us -> 10.6 us  [half_back(): d_normed = lax.psum(total.astype(jnp.bfloat16), 'tp').astype(jnp.float32)]
    another operation x0 -> x4, other arithmetic: none -> 7.53 us  [exchange_gather(): shards = jnp.stack([array for _ in range(devices)])]
  transfers between devices with their start and end apart: 11 -> 11, of which waited for: 11 -> 8; matrix products, arithmetic and copies ran while one was open for 6% -> 8% of each run, Pallas kernels for 0% -> 0%
where the time goes in v1:
time: 554 us; the launch traced here: 553 us
  waiting for transfers between devices  396 us (71%)
  matrix products  56.5 us (10%)
  blocking collectives  31.5 us (6%)
  other arithmetic  25.2 us (5%)
  starting transfers between devices  21.3 us (4%)
  between operations  14 us (3%)
  local copies, waits for them, and re-layouts  8.77 us (2%)
    all_gather x2, waiting for transfers between devices, gathered(): return lax.all_gather(own, 'fs', axis=0, tiled=True)  218 us
    reduce_scatter x1, waiting for transfers between devices, on_device(): lax.psum_scatter((0.5 * partial).astype(jnp.bfloat16), 'fs', scatter_dime...  75.5 us
    all_to_all x4, waiting for transfers between devices, exchange_gather(): shards = lax.all_to_all(shards, mesh_axis, split_axis=0, concat_axis=0)  45.8 us
    ppermute x2, waiting for transfers between devices, half_back(): got = lax.ppermute(sent, 'rep', [(i, (i + k) % reps) for i in range(reps)])  45.6 us
    psum x1, blocking collectives, on_device(): norms = lax.psum(jnp.sum(grad * grad, axis=0), 'fs')  20.5 us
    all_to_all x4, starting transfers between devices, exchange_gather(): shards = lax.all_to_all(shards, mesh_axis, split_axis=0, concat_axis=0)  17.8 us
    dot_general x2, matrix products, half_back(): lax.dot_general(d_gate, gates, dims, preferred_element_type=jnp.float32)  14 us
  transfers between devices with their start and end apart: 11, of which 8 were waited for; matrix products, arithmetic and copies ran while one was open for 8% of the time, Pallas kernels for 0%

profile of v1, /device:TPU:0, one launch (start us, length us, event | category | flops | bytes accessed | tf_op | source)
XLA Modules:
  0.0 553.0 jit_solution(5039791954245912608)
XLA Ops:
  12.0 4.2 all-to-all-start.1
  19.3 22.8 %all-to-all-done.1 = bf16[2,256,2048]{2,1,0:T(8,128)(2,1)S(1)} async-done(((bf16[2,256,2048]{2,1,0:T(8,128)(2,1)}), bf16[2,256,2048]{2,1,0:T(8,128)(2,1)S(1)}, u32[]{:S(2)}, u32[]{:S(2)}) %all-to-all-start.1) | async-done | bytes 2097184 | tf_op jit(solution)/shard_map/all_to_all | solution.py:12
  42.1 4.8 all-to-all-start
  49.2 101.9 %all-gather.3.cloned.1.call-done = bf16[2048,2304]{0,1:T(8,128)(2,1)} async-done(((bf16[256,2304]{0,1:T(8,128)(2,1)}), bf16[2048,2304]{0,1:T(8,128)(2,1)}) %all-gather.3.cloned.1.call-update) | async-done | bytes 9437200 | tf_op jit(solution)/shard_map/all_gather | solution.py:27
  151.1 5.5 fusion.15
  156.6 5.7 %fusion.36 = f32[512,768]{1,0:T(8,128)} fusion(bf16[512,2048]{1,0:T(8,128)(2,1)} %bitcast.1, bf16[2048,2304]{0,1:T(8,128)(2,1)} %all-gather.3.cloned.1.call-done), kind=kOutput, calls=%fused_computation.64 | convolution fusion | flops 1611005952 | bytes 6815744 | tf_op jit(solution)/shard_map/dot_general | solution.py:39
  162.3 9.9 %fusion.13 = f32[512,2048]{1,0:T(8,128)} fusion(bf16[2048,2304]{0,1:T(8,128)(2,1)} %all-gather.3.cloned.1.call-done, f32[512,768]{1,0:T(8,128)} %fusion.15, f32[512,768]{1,0:T(8,128)} %fusion.36, bf16[512,2048]{1,0:T(8,128)(2,1)S(1)} %copy-done.8), kind=kOutput, calls=%fused_computation.20 | convolution fusion | flops 3225157632 | bytes 15728640 | tf_op jit(solution)/shard_map/dot_general | solution.py:46
  172.1 5.9 %add_convert_fusion.1 = bf16[512,2048]{1,0:T(8,128)(2,1)S(1)} fusion(f32[512,2048]{1,0:T(8,128)} %fusion.13, bf16[2048,2304]{0,1:T(8,128)(2,1)} %all-gather.3.cloned.1.call-done, f32[512,768]{1,0:T(8,128)} %fusion.36, f32[512,768]{1,0:T(8,128)} %fusion.15), kind=kOutput, calls=%fused_computation.7 | convolution fusion | flops 1615069184 | bytes 12582912 | tf_op jit(solution)/shard_map/dot_general | solution.py:47
  180.6 22.9 %collective-permute-done = bf16[256,2048]{1,0:T(8,128)(2,1)} collective-permute-done((bf16[256,2048]{1,0:T(8,128)(2,1)}, bf16[256,2048]{1,0:T(8,128)(2,1)}, u32[]{:S(2)}, u32[]{:S(2)}) %collective-permute-start) | collective-permute-done | bytes 1048608 | tf_op jit(solution)/shard_map/ppermute | solution.py:58
  211.4 3.9 all-to-all-start.3
  215.7 23.1 %all-to-all-done.3 = bf16[2,256,2048]{2,1,0:T(8,128)(2,1)S(1)} async-done(((bf16[2,256,2048]{2,1,0:T(8,128)(2,1)}), bf16[2,256,2048]{2,1,0:T(8,128)(2,1)S(1)}, u32[]{:S(2)}, u32[]{:S(2)}) %all-to-all-start.3) | async-done | bytes 2097184 | tf_op jit(solution)/shard_map/all_to_all | solution.py:12
  245.1 4.8 all-to-all-start.2
  250.0 116.3 %all-gather.5.cloned.1.call-done = bf16[2048,2304]{0,1:T(8,128)(2,1)} async-done(((bf16[256,2304]{0,1:T(8,128)(2,1)}), bf16[2048,2304]{0,1:T(8,128)(2,1)}) %all-gather.5.cloned.1.call-update) | async-done | bytes 9437200 | tf_op jit(solution)/shard_map/all_gather | solution.py:27
  366.3 5.5 fusion.8
  371.8 5.5 fusion.11
  377.3 4.5 fusion.39
  381.8 4.2 fusion.6
  386.0 3.8 add_convert_fusion
  391.5 22.6 %collective-permute-done.1 = bf16[256,2048]{1,0:T(8,128)(2,1)S(1)} collective-permute-done((bf16[256,2048]{1,0:T(8,128)(2,1)S(1)}, bf16[256,2048]{1,0:T(8,128)(2,1)S(1)}, u32[]{:S(2)}, u32[]{:S(2)}) %collective-permute-start.1) | collective-permute-done | bytes 1048608 | tf_op jit(solution)/shard_map/ppermute | solution.py:58
  415.8 6.1 %multiply_convert_fusion = bf16[2048,768]{1,0:T(8,128)(2,1)} fusion(bf16[512,2048]{1,0:T(8,128)(2,1)} %bitcast.6, f32[512,768]{1,0:T(8,128)} %fusion.11, f32[512,768]{1,0:T(8,128)} %fusion.8), kind=kOutput, calls=%fused_computation | convolution fusion | flops 1616117760 | bytes 8388608 | tf_op jit(solution)/shard_map/dot_general | solution.py:90
  423.5 10.6 %all-reduce.5.cloned.1.call-done = bf16[256,2048]{1,0:T(8,128)(2,1)} async-done(((bf16[256,2048]{1,0:T(8,128)(2,1)}), bf16[256,2048]{1,0:T(8,128)(2,1)}) %all-reduce.5.cloned.1.call-update) | async-done | bytes 1048592 | tf_op jit(solution)/shard_map/psum | solution.py:60
  437.5 75.5 %reduce-scatter.2.cloned.1.call-done = bf16[256,768]{1,0:T(8,128)(2,1)} async-done(((bf16[2048,768]{1,0:T(8,128)(2,1)}), bf16[256,768]{1,0:T(8,128)(2,1)}) %reduce-scatter.2.cloned.1.call-update) | async-done | bytes 393232 | tf_op jit(solution)/shard_map/reduce_scatter | solution.py:93
  513.0 11.0 %all_gather.11 = bf16[256,1536]{1,0:T(8,128)(2,1)S(1)} all-gather(bf16[256,768]{1,0:T(8,128)(2,1)} %reduce-scatter.2.cloned.1.call-done), channel_id=1, replica_groups=mesh['rep'=2,'fs'=8,'tp'=2] {'rep'}, dimensions={1}, use_global_device_ids=true | all-gather | bytes 1179648 | tf_op jit(solution)/shard_map/all_gather | solution.py:96
  526.0 20.5 %psum.23 = f32[1536]{0:T(1024)} all-reduce(f32[1536]{0:T(1024)S(1)} %fusion.32), channel_id=1, replica_groups=mesh['rep'=2,'fs'=8,'tp'=2] {'fs'}, use_global_device_ids=true, to_apply=%region_10.0 | all-reduce | flops 1536 | bytes 12288 | tf_op jit(solution)/shard_map/psum | solution.py:97
  (76 shorter events, 37.6 us)
Async XLA Ops:
  7.2 1.7 copy-start
  7.2 143.9 %all-gather.3.cloned.1.call-start = ((), (), s32[]{:S(2)}) async-start(), calls=%async_computation.5 | async-start | bytes 10616832 | tf_op jit(solution)/shard_map/all_gather | solution.py:27
  8.8 1.7 copy-start.2
  12.0 30.1 %all-to-all-start.1 = ((bf16[2,256,2048]{2,1,0:T(8,128)(2,1)}), bf16[2,256,2048]{2,1,0:T(8,128)(2,1)S(1)}, u32[]{:S(2)}, u32[]{:S(2)}) async-start(bf16[2,256,2048]{2,1,0:T(8,128)(2,1)} %pad_maximum_fusion.1), calls=%async_computation.1 | async-start | bytes 4194304 | tf_op jit(solution)/shard_map/all_to_all | solution.py:12
  42.1 114.5 %all-to-all-start = ((bf16[2,256,2048]{2,1,0:T(8,128)(2,1)}), bf16[2,256,2048]{2,1,0:T(8,128)(2,1)}, u32[]{:S(2)}, u32[]{:S(2)}) async-start(bf16[2,256,2048]{2,1,0:T(8,128)(2,1)} %pad_maximum_fusion), calls=%async_computation | async-start | bytes 4194304 | tf_op jit(solution)/shard_map/all_to_all | solution.py:12
  46.9 194.2 %all-reduce.3.cloned.1.call-start = ((), (), s32[]{:S(2)}) async-start(), calls=%async_computation.6 | async-start | bytes 2097152 | tf_op jit(solution)/shard_map/psum | solution.py:60
  156.6 5.7 %copy-start.8 = (bf16[512,2048]{1,0:T(8,128)(2,1)S(1)}, bf16[512,2048]{1,0:T(8,128)(2,1)}, u32[]{:S(2)}) copy-start(bf16[512,2048]{1,0:T(8,128)(2,1)} %fusion.1) | copy-start | bytes 6291460
  179.1 24.4 %collective-permute-start = (bf16[256,2048]{1,0:T(8,128)(2,1)}, bf16[256,2048]{1,0:T(8,128)(2,1)}, u32[]{:S(2)}, u32[]{:S(2)}) collective-permute-start(bf16[256,2048]{1,0:T(8,128)(2,1)} %constant_dynamic-slice_fusion.3), channel_id=1, source_target_pairs={{0,16},{16,0},{1,17},{17,1},{2,18},{18,2},{3,19},{19,3},{4,20},{20... | collective-permute-start | bytes 3145736 | tf_op jit(solution)/shard_map/ppermute | solution.py:58
  206.1 160.2 %all-gather.5.cloned.1.call-start = ((), (), s32[]{:S(2)}) async-start(), calls=%async_computation.7 | async-start | bytes 10616832 | tf_op jit(solution)/shard_map/all_gather | solution.py:27
  207.7 2.2 copy-start.3
  211.4 27.3 %all-to-all-start.3 = ((bf16[2,256,2048]{2,1,0:T(8,128)(2,1)}), bf16[2,256,2048]{2,1,0:T(8,128)(2,1)S(1)}, u32[]{:S(2)}, u32[]{:S(2)}) async-start(bf16[2,256,2048]{2,1,0:T(8,128)(2,1)} %pad_maximum_fusion.3), calls=%async_computation.3 | async-start | bytes 4194304 | tf_op jit(solution)/shard_map/all_to_all | solution.py:12
  241.1 1.9 copy-start.5
  241.1 1.9 copy-start.6
  245.1 132.1 %all-to-all-start.2 = ((bf16[2,256,2048]{2,1,0:T(8,128)(2,1)}), bf16[2,256,2048]{2,1,0:T(8,128)(2,1)}, u32[]{:S(2)}, u32[]{:S(2)}) async-start(bf16[2,256,2048]{2,1,0:T(8,128)(2,1)} %pad_maximum_fusion.2), calls=%async_computation.2 | async-start | bytes 4194304 | tf_op jit(solution)/shard_map/all_to_all | solution.py:12
  250.0 184.1 %all-reduce.5.cloned.1.call-start = ((), (), s32[]{:S(2)}) async-start(), calls=%async_computation.8 | async-start | bytes 2097152 | tf_op jit(solution)/shard_map/psum | solution.py:60
  377.3 4.5 copy-start.9
  377.3 4.5 copy-start.10
  389.9 24.2 %collective-permute-start.1 = (bf16[256,2048]{1,0:T(8,128)(2,1)S(1)}, bf16[256,2048]{1,0:T(8,128)(2,1)S(1)}, u32[]{:S(2)}, u32[]{:S(2)}) collective-permute-start(bf16[256,2048]{1,0:T(8,128)(2,1)S(1)} %constant_dynamic-slice_fusion), channel_id=1, source_target_pairs={{0,16},{16,0},{1,17},{17,1},{2,18},{18,2},{3,19},{19,3},{4,20},{20... | collective-permute-start | bytes 3145736 | tf_op jit(solution)/shard_map/ppermute | solution.py:58
  415.5 97.5 %reduce-scatter.2.cloned.1.call-start = ((), (), s32[]{:S(2)}) async-start(), calls=%async_computation.9 | async-start | bytes 3538944 | tf_op jit(solution)/shard_map/reduce_scatter | solution.py:93
  421.9 1.3 copy-start.4
  434.1 1.8 copy-start.7
  524.0 22.5 %copy-start.1 = (bf16[1536,256]{1,0:T(8,128)(2,1)S(1)}, bf16[1536,256]{1,0:T(8,128)(2,1)}, u32[]{:S(2)}) copy-start(bf16[1536,256]{1,0:T(8,128)(2,1)} %param.17) | copy-start | bytes 2359300
Sparse Core Ops, SparseCore 0:
  10.6 140.4 all-gather.2
  206.3 18.4 all-reduce.2
  227.3 138.9 all-gather.4
  415.6 18.4 all-reduce.4
  437.5 75.4 reduce-scatter.1
